TPU v7x, 32 devices: a whole 2x2x4 slice. The times are simulated.
32 devices in a mesh: grp: 2 (over y), fs: 4 (over z), tp: 4 (over x, core).
Axes of the slice: x: 2, y: 2, z: 4, core: 2. Of those that a mesh axis runs over, the one named last changes fastest.
Arguments:
- tokens: bfloat16 [2048, 2048], P(('grp', 'fs')), parts along dimension 0, may hold values from -6 to 6
- ffn_pre_gain: bfloat16 [2048], replicated, may hold values from 0.099609375 to 1.8984375
- gate_weight: bfloat16 [2048, 5632], P('fs', 'tp'), may hold values from -0.125 to 0.125
- up_weight: bfloat16 [2048, 5632], P('fs', 'tp'), may hold values from -0.125 to 0.125
- down_weight: bfloat16 [5632, 2048], P('tp', 'fs'), may hold values from -0.078125 to 0.078125
- ffn_post_gain: bfloat16 [2048], replicated, may hold values from 0.099609375 to 1.8984375
- mix_pre_gain: bfloat16 [2048], replicated, may hold values from 0.099609375 to 1.8984375
- mix_u_weight: bfloat16 [2048, 2048], P('fs', 'tp'), may hold values from -0.125 to 0.125
- mix_v_weight: bfloat16 [2048, 2048], P('fs', 'tp'), may hold values from -0.125 to 0.125
- spatial_gain: bfloat16 [2048], P('tp'), may hold values from 0.099609375 to 1.8984375
- spatial_weight: bfloat16 [16, 128, 128], P('tp'), may hold values from -0.5 to 0.5
- spatial_bias: bfloat16 [16, 128], P('tp'), may hold values from 0.099609375 to 1.8984375
- mix_out_weight: bfloat16 [2048, 2048], P('tp', 'fs'), may hold values from -0.125 to 0.125
- mix_post_gain: bfloat16 [2048], replicated, may hold values from 0.099609375 to 1.8984375
- late_pre_gain: bfloat16 [2048], replicated, may hold values from 0.099609375 to 1.8984375
- late_post_gain: bfloat16 [2048], replicated, may hold values from 0.099609375 to 1.8984375
Outputs:
- result: bfloat16 [2048, 2048], P(('grp', 'fs')), parts along dimension 0
There are 2 independent parts, one for each index of `grp`. A program takes and returns all parts, laid end to end along the dimension named above; an argument that names none is the same for every part. Nothing has to cross between parts.
All inputs are finite; a program needn't handle non-finite values.
Results may differ from a plain program's by a relative error of at most 0.019.
Values may be sent and summed in bfloat16 or wider, within the bound.
No kernel may reach another device: no remote copies, remote signals or barrier semaphores. Data moves between devices by JAX's collectives and lax.ppermute only.
A program may use at most 128 MiB of HBM per device.

v0:
```python
import jax
import jax.numpy as jnp
from jax import lax
from jax.sharding import PartitionSpec as P

GROUP_WIDTH = 128
BLOCK = 128


def row_norm(values, gain):
    scale = lax.rsqrt(jnp.mean(values * values, axis=-1, keepdims=True) + 1e-06)
    return values * scale * gain.astype(jnp.float32)


def reduce_partial(terms):
    return lax.psum(terms.astype(jnp.bfloat16), "tp").astype(jnp.float32)


def add_branch(stream, terms, gain, factor):
    total = reduce_partial(terms)
    return (stream.astype(jnp.float32) + factor * row_norm(total, gain)).astype(jnp.bfloat16)


def gated_hidden(normed, gate_full, up_full):
    gate = jnp.dot(normed, gate_full, preferred_element_type=jnp.float32)
    upper = jnp.dot(normed, up_full, preferred_element_type=jnp.float32)
    return (jax.nn.silu(gate) * upper).astype(jnp.bfloat16)


def spatial_mix(u_linear, v_linear, spatial_gain, spatial_weight, spatial_bias):
    count = u_linear.shape[0]
    gated_u = jax.nn.gelu(u_linear, approximate=False)
    gating_v = jax.nn.gelu(v_linear, approximate=False)
    groups = gating_v.shape[1] // GROUP_WIDTH
    grouped = gating_v.reshape(count, groups, GROUP_WIDTH)
    centred = grouped - jnp.mean(grouped, axis=-1, keepdims=True)
    vnorm = centred * lax.rsqrt(jnp.mean(centred * centred, axis=-1, keepdims=True) + 1e-05)
    vnorm = (vnorm * spatial_gain.astype(jnp.float32).reshape(groups, GROUP_WIDTH)).astype(
        jnp.bfloat16
    )
    blocks = vnorm.reshape(count // BLOCK, BLOCK, groups, GROUP_WIDTH)
    lower = jnp.tril(jnp.ones((BLOCK, BLOCK), dtype=bool))
    masked = jnp.where(lower[None], spatial_weight, jnp.zeros_like(spatial_weight))
    spatial = jnp.einsum("gts,nsgc->ntgc", masked, blocks, preferred_element_type=jnp.float32)
    spatial = spatial + spatial_bias.astype(jnp.float32).T[None, :, :, None]
    return (gated_u * spatial.reshape(count, groups * GROUP_WIDTH)).astype(jnp.bfloat16)


def shards(
    tokens,
    ffn_pre_gain,
    gate_weight,
    up_weight,
    down_weight,
    ffn_post_gain,
    mix_pre_gain,
    mix_u_weight,
    mix_v_weight,
    spatial_gain,
    spatial_weight,
    spatial_bias,
    mix_out_weight,
    mix_post_gain,
    late_pre_gain,
    late_post_gain,
):
    normed = row_norm(tokens.astype(jnp.float32), ffn_pre_gain).astype(jnp.bfloat16)
    gate_full, up_full = (
        lax.all_gather(gate_weight, "fs", axis=0, tiled=True),
        lax.all_gather(up_weight, "fs", axis=0, tiled=True),
    )
    down_full = lax.all_gather(down_weight, "fs", axis=1, tiled=True)
    hidden = gated_hidden(normed, gate_full, up_full)
    terms = jnp.dot(hidden, down_full, preferred_element_type=jnp.float32)
    first = add_branch(tokens, terms, ffn_post_gain, 0.5)
    normed = row_norm(first.astype(jnp.float32), mix_pre_gain).astype(jnp.bfloat16)
    u_full, v_full = (
        lax.all_gather(mix_u_weight, "fs", axis=0, tiled=True),
        lax.all_gather(mix_v_weight, "fs", axis=0, tiled=True),
    )
    u_linear = jnp.dot(normed, u_full, preferred_element_type=jnp.float32)
    v_linear = jnp.dot(normed, v_full, preferred_element_type=jnp.float32)
    mixed = spatial_mix(u_linear, v_linear, spatial_gain, spatial_weight, spatial_bias)
    out_full = lax.all_gather(mix_out_weight, "fs", axis=1, tiled=True)
    terms = jnp.dot(mixed, out_full, preferred_element_type=jnp.float32)
    second = add_branch(first, terms, mix_post_gain, 1.0)
    normed = row_norm(second.astype(jnp.float32), late_pre_gain).astype(jnp.bfloat16)
    hidden = gated_hidden(normed, gate_full, up_full)
    terms = jnp.dot(hidden, down_full, preferred_element_type=jnp.float32)
    return add_branch(second, terms, late_post_gain, 0.5)


def solution(mesh):
    in_specs = (
        P(("grp", "fs"), None),
        P(),
        P("fs", "tp"),
        P("fs", "tp"),
        P("tp", "fs"),
        P(),
        P(),
        P("fs", "tp"),
        P("fs", "tp"),
        P("tp"),
        P("tp", None, None),
        P("tp", None),
        P("tp", "fs"),
        P(),
        P(),
        P(),
    )
    out_specs = P(("grp", "fs"), None)
    return jax.shard_map(shards, mesh=mesh, in_specs=in_specs, out_specs=out_specs, check_vma=False)
```

profile of v0, /device:TPU:0, one launch (start us, length us, event | category | flops | bytes accessed | tf_op | source)
XLA Modules:
  0.0 620.2 jit_solution(5151979985591970159)
XLA Ops:
  6.5 0.0 copy-start.2
  6.5 0.0 copy-start
  6.5 0.0 all-gather.7.cloned.1.call-start
  6.5 0.7 all-gather.7.cloned.1.call-update
  7.3 0.0 all-gather.11.cloned.1.call-start
  7.3 0.7 all-gather.11.cloned.1.call-update
  8.0 0.0 all-gather.9.cloned.1.call-start
  8.1 0.7 all-gather.9.cloned.1.call-update
  8.7 0.0 all-reduce.4.cloned.1.call-start
  8.8 0.0 copy-done.2
  8.8 0.0 copy-done
  8.8 0.3 fusion.10
  9.1 109.2 %all-gather.7.cloned.1.call-done = bf16[2048,1408]{1,0:T(8,128)(2,1)} async-done(((bf16[512,1408]{1,0:T(8,128)(2,1)}), bf16[2048,1408]{1,0:T(8,128)(2,1)}) %all-gather.7.cloned.1.call-update) | async-done | bytes 5767184 | tf_op jit(solution)/shard_map/all_gather | solution.py:69
  118.3 4.5 fusion.59
  122.8 102.0 %all-gather.11.cloned.1.call-done = bf16[1408,2048]{1,0:T(8,128)(2,1)} async-done(((bf16[1408,512]{1,0:T(8,128)(2,1)}), bf16[1408,2048]{1,0:T(8,128)(2,1)}) %all-gather.11.cloned.1.call-update) | async-done | bytes 5767184 | tf_op jit(solution)/shard_map/all_gather | solution.py:72
  224.9 106.6 %all-gather.9.cloned.1.call-done = bf16[2048,1408]{1,0:T(8,128)(2,1)} async-done(((bf16[512,1408]{1,0:T(8,128)(2,1)}), bf16[2048,1408]{1,0:T(8,128)(2,1)}) %all-gather.9.cloned.1.call-update) | async-done | bytes 5767184 | tf_op jit(solution)/shard_map/all_gather | solution.py:70
  331.4 8.9 %convolution_convert_fusion.2 = bf16[256,2048]{1,0:T(8,128)(2,1)} fusion(bf16[1408,2048]{1,0:T(8,128)(2,1)} %all-gather.11.cloned.1.call-done, bf16[2048,1408]{1,0:T(8,128)(2,1)} %all-gather.9.cloned.1.call-done, f32[256,1408]{1,0:T(8,128)S(1)} %fusion.59, bf16[256,2048]{1,0:T(8,128)(2,1)S(1)} %copy-done, f32[2048]{0:T(1024)S(1)} %convert_element_type.82, ...), kind=kOutput, calls=%fused_computation.21 | convolution fusion | flops 2957574144 | bytes 15082496 | tf_op jit(solution)/shard_map/dot_general | solution.py:74
  340.4 0.0 copy-start.3
  340.4 0.0 all-reduce.4.cloned.1.call-update
  340.4 0.0 all-gather.15.cloned.1.call-start
  340.5 0.5 all-gather.15.cloned.1.call-update
  341.0 0.0 all-gather.13.cloned.1.call-start
  341.0 0.5 all-gather.13.cloned.1.call-update
  341.6 0.0 all-gather.17.cloned.1.call-start
  341.6 0.7 all-gather.17.cloned.1.call-update
  342.3 0.2 all-reduce.6.cloned.1.call-start
  342.6 0.0 copy-done.3
  342.6 0.0 copy-done.4
  342.6 0.0 copy-done.8
  342.6 0.0 copy-done.9
  342.7 32.4 %all-reduce.4.cloned.1.call-done = bf16[256,2048]{1,0:T(8,128)(2,1)} async-done(((bf16[256,2048]{1,0:T(8,128)(2,1)}), bf16[256,2048]{1,0:T(8,128)(2,1)}) %all-reduce.4.cloned.1.call-update) | async-done | bytes 1048592 | tf_op jit(solution)/shard_map/psum | solution.py:16
  375.1 1.5 fusion.2
  376.6 2.0 fusion.14
  378.6 44.1 %all-gather.15.cloned.1.call-done = bf16[2048,512]{1,0:T(8,128)(2,1)} async-done(((bf16[512,512]{1,0:T(8,128)(2,1)}), bf16[2048,512]{1,0:T(8,128)(2,1)}) %all-gather.15.cloned.1.call-update) | async-done | bytes 2097168 | tf_op jit(solution)/shard_map/all_gather | solution.py:79
  422.7 3.4 fusion.28
  426.1 0.2 reshape.99
  426.3 0.0 copy-start.1
  426.3 0.2 reshape.98
  426.5 0.3 reduce_sum.75
  426.8 0.6 multiply_reduce_fusion
  427.5 0.1 copy.36
  427.6 0.1 copy.37
  427.7 0.2 copy.25
  427.9 0.0 copy-done.1
  427.9 0.3 fusion.22
  428.2 0.2 copy.28
  428.5 40.1 %all-gather.13.cloned.1.call-done = bf16[2048,512]{1,0:T(8,128)(2,1)} async-done(((bf16[512,512]{1,0:T(8,128)(2,1)}), bf16[2048,512]{1,0:T(8,128)(2,1)}) %all-gather.13.cloned.1.call-update) | async-done | bytes 2097168 | tf_op jit(solution)/shard_map/all_gather | solution.py:78
  468.6 46.1 %all-gather.17.cloned.1.call-done = bf16[512,2048]{1,0:T(8,128)(2,1)} async-done(((bf16[512,512]{1,0:T(8,128)(2,1)}), bf16[512,2048]{1,0:T(8,128)(2,1)}) %all-gather.17.cloned.1.call-update) | async-done | bytes 2097168 | tf_op jit(solution)/shard_map/all_gather | solution.py:84
  514.7 5.7 convolution_convert_fusion
  520.4 0.0 all-reduce.6.cloned.1.call-update
  520.4 0.3 all-reduce.8.cloned.1.call-start
  520.7 0.0 copy-done.5
  520.7 0.0 copy-done.6
  520.7 34.9 %all-reduce.6.cloned.1.call-done = bf16[256,2048]{1,0:T(8,128)(2,1)} async-done(((bf16[256,2048]{1,0:T(8,128)(2,1)}), bf16[256,2048]{1,0:T(8,128)(2,1)}) %all-reduce.6.cloned.1.call-update) | async-done | bytes 1048592 | tf_op jit(solution)/shard_map/psum | solution.py:16
  555.7 1.5 fusion.5
  557.2 1.9 fusion.18
  559.1 4.5 fusion.45
  563.6 0.0 copy-start.7
  563.6 8.9 %convolution_convert_fusion.1 = bf16[256,2048]{1,0:T(8,128)(2,1)} fusion(bf16[1408,2048]{1,0:T(8,128)(2,1)} %all-gather.11.cloned.1.call-done, bf16[2048,1408]{1,0:T(8,128)(2,1)} %all-gather.9.cloned.1.call-done, f32[256,1408]{1,0:T(8,128)S(1)} %fusion.45, bf16[256,2048]{1,0:T(8,128)(2,1)S(1)} %get-tuple-element.6, f32[2048]{0:T(1024)S(1)} %convert_element_type.99, ...), kind=kOutput, calls=%fused_computation.20 | convolution fusion | flops 2957574144 | bytes 15082496 | tf_op jit(solution)/shard_map/dot_general | solution.py:89
  572.5 0.0 all-reduce.8.cloned.1.call-update
  572.5 0.0 copy-done.7
  572.5 36.9 %all-reduce.8.cloned.1.call-done = bf16[256,2048]{1,0:T(8,128)(2,1)} async-done(((bf16[256,2048]{1,0:T(8,128)(2,1)}), bf16[256,2048]{1,0:T(8,128)(2,1)}) %all-reduce.8.cloned.1.call-update) | async-done | bytes 1048592 | tf_op jit(solution)/shard_map/psum | solution.py:16
  609.4 1.5 fusion.7
  610.9 2.8 fusion.21
  (22 shorter events, 0.1 us)
Async XLA Ops:
  6.5 2.3 copy-start.2
  6.5 2.3 copy-start
  6.5 111.8 %all-gather.7.cloned.1.call-start = ((), (), s32[]{:S(2)}) async-start(), calls=%async_computation | async-start | bytes 7208960 | tf_op jit(solution)/shard_map/all_gather | solution.py:69
  7.3 217.6 %all-gather.11.cloned.1.call-start = ((), (), s32[]{:S(2)}) async-start(), calls=%async_computation.2 | async-start | bytes 7208960 | tf_op jit(solution)/shard_map/all_gather | solution.py:72
  8.0 323.4 %all-gather.9.cloned.1.call-start = ((), (), s32[]{:S(2)}) async-start(), calls=%async_computation.1 | async-start | bytes 7208960 | tf_op jit(solution)/shard_map/all_gather | solution.py:70
  8.7 366.4 %all-reduce.4.cloned.1.call-start = ((), (), s32[]{:S(2)}) async-start(), calls=%async_computation.3 | async-start | bytes 2097152 | tf_op jit(solution)/shard_map/psum | solution.py:16
  340.4 2.2 copy-start.3
  340.4 2.2 copy-start.4
  340.4 2.2 copy-start.8
  340.4 2.3 copy-start.9
  340.4 82.3 %all-gather.15.cloned.1.call-start = ((), (), s32[]{:S(2)}) async-start(), calls=%async_computation.5 | async-start | bytes 2621440 | tf_op jit(solution)/shard_map/all_gather | solution.py:79
  341.0 127.6 %all-gather.13.cloned.1.call-start = ((), (), s32[]{:S(2)}) async-start(), calls=%async_computation.4 | async-start | bytes 2621440 | tf_op jit(solution)/shard_map/all_gather | solution.py:78
  341.6 173.1 %all-gather.17.cloned.1.call-start = ((), (), s32[]{:S(2)}) async-start(), calls=%async_computation.6 | async-start | bytes 2621440 | tf_op jit(solution)/shard_map/all_gather | solution.py:84
  342.3 213.3 %all-reduce.6.cloned.1.call-start = ((), (), s32[]{:S(2)}) async-start(), calls=%async_computation.7 | async-start | bytes 2097152 | tf_op jit(solution)/shard_map/psum | solution.py:16
  426.3 1.7 copy-start.1
  514.7 6.0 copy-start.5
  514.7 6.0 copy-start.6
  520.4 89.0 %all-reduce.8.cloned.1.call-start = ((), (), s32[]{:S(2)}) async-start(), calls=%async_computation.8 | async-start | bytes 2097152 | tf_op jit(solution)/shard_map/psum | solution.py:16
  563.6 9.0 %copy-start.7 = (bf16[2048]{0:T(1024)(128)(2,1)S(1)}, bf16[2048]{0:T(1024)(128)(2,1)}, u32[]{:S(2)}) copy-start(bf16[2048]{0:T(1024)(128)(2,1)} %param.31) | copy-start | bytes 12292
Sparse Core Ops, SparseCore 0:
  8.9 109.3 all-gather.6
  119.9 104.9 all-gather.10
  226.5 104.9 all-gather.8
  340.5 34.5 all-reduce.3
  376.5 46.1 all-gather.14
  424.1 44.4 all-gather.12
  470.2 44.4 all-gather.16
  520.5 35.0 all-reduce.5
  572.6 36.7 all-reduce.7
where the time goes:
time: 621 us; the launch traced here: 620 us
  waiting for transfers between devices  556 us (90%)
  matrix products  36.2 us (6%)
  between operations  13.5 us (2%)
  other arithmetic  12.6 us (2%)
    all_gather x1, waiting for transfers between devices, shards(): lax.all_gather(gate_weight, 'fs', axis=0, tiled=True)  109 us
    all_gather x1, waiting for transfers between devices, shards(): lax.all_gather(up_weight, 'fs', axis=0, tiled=True)  107 us
    psum x3, waiting for transfers between devices, reduce_partial(): return lax.psum(terms.astype(jnp.bfloat16), 'tp').astype(jnp.float32)  104 us
    all_gather x1, waiting for transfers between devices, shards(): down_full = lax.all_gather(down_weight, 'fs', axis=1, tiled=True)  102 us
    all_gather x1, waiting for transfers between devices, shards(): out_full = lax.all_gather(mix_out_weight, 'fs', axis=1, tiled=True)  46.1 us
    all_gather x1, waiting for transfers between devices, shards(): lax.all_gather(mix_v_weight, 'fs', axis=0, tiled=True)  44.1 us
    all_gather x1, waiting for transfers between devices, shards(): lax.all_gather(mix_u_weight, 'fs', axis=0, tiled=True)  40.1 us
    dot_general x2, matrix products, shards(): terms = jnp.dot(hidden, down_full, preferred_element_type=jnp.float32)  17.8 us
  transfers between devices with their start and end apart: 9, of which 9 were waited for; matrix products, arithmetic and copies ran while one was open for 2% of the time, Pallas kernels for 0%

commit v1 on v0

--- a/solution.py
+++ b/solution.py
@@ -69,7 +69,7 @@
         lax.all_gather(gate_weight, "fs", axis=0, tiled=True),
         lax.all_gather(up_weight, "fs", axis=0, tiled=True),
     )
-    down_full = lax.all_gather(down_weight, "fs", axis=1, tiled=True)
+    down_full = jnp.concatenate(lax.all_gather(down_weight, "fs"), 1)
     hidden = gated_hidden(normed, gate_full, up_full)
     terms = jnp.dot(hidden, down_full, preferred_element_type=jnp.float32)
     first = add_branch(tokens, terms, ffn_post_gain, 0.5)

time: 621 us -> 621 us (level)
  local copies, waits for them, and re-layouts: 1.03 us -> 9.44 us
  waiting for transfers between devices: 556 us -> 548 us
    all_gather x1, waiting for transfers between devices: 109 us -> 98.1 us  [shards(): lax.all_gather(gate_weight, 'fs', axis=0, tiled=True)]
    reshape x0 -> x1, local copies, waits for them, and re-layouts: none -> 8.42 us  [shards(): down_full = jnp.concatenate(lax.all_gather(down_weight, 'fs'), 1)]
    all_gather x1, waiting for transfers between devices: 102 us -> 109 us  [shards(): down_full = jnp.concatenate(lax.all_gather(down_weight, 'fs'), 1)]
  transfers between devices with their start and end apart: 9 -> 9, of which waited for: 9 -> 9; matrix products, arithmetic and copies ran while one was open for 2% -> 4% of each run, Pallas kernels for 0% -> 0%
where the time goes in v1:
time: 621 us; the launch traced here: 620 us
  waiting for transfers between devices  548 us (88%)
  matrix products  36 us (6%)
  between operations  13.5 us (2%)
  other arithmetic  12.5 us (2%)
  local copies, waits for them, and re-layouts  9.44 us (2%)
    all_gather x1, waiting for transfers between devices, shards(): down_full = jnp.concatenate(lax.all_gather(down_weight, 'fs'), 1)  109 us
    psum x3, waiting for transfers between devices, reduce_partial(): return lax.psum(terms.astype(jnp.bfloat16), 'tp').astype(jnp.float32)  104 us
    all_gather x1, waiting for transfers between devices, shards(): lax.all_gather(up_weight, 'fs', axis=0, tiled=True)  102 us
    all_gather x1, waiting for transfers between devices, shards(): lax.all_gather(gate_weight, 'fs', axis=0, tiled=True)  98.1 us
    all_gather x1, waiting for transfers between devices, shards(): out_full = lax.all_gather(mix_out_weight, 'fs', axis=1, tiled=True)  46.1 us
    all_gather x1, waiting for transfers between devices, shards(): lax.all_gather(mix_v_weight, 'fs', axis=0, tiled=True)  44.1 us
    all_gather x1, waiting for transfers between devices, shards(): lax.all_gather(mix_u_weight, 'fs', axis=0, tiled=True)  40.2 us
    dot_general x2, matrix products, shards(): terms = jnp.dot(hidden, down_full, preferred_element_type=jnp.float32)  17.7 us
  transfers between devices with their start and end apart: 9, of which 9 were waited for; matrix products, arithmetic and copies ran while one was open for 4% of the time, Pallas kernels for 0%

profile of v1, /device:TPU:0, one launch (start us, length us, event | category | flops | bytes accessed | tf_op | source)
XLA Modules:
  0.0 620.1 jit_solution(16838903782644297452)
XLA Ops:
  6.5 0.0 copy-start.2
  6.5 0.0 copy-start
  6.5 0.0 all-gather.18.cloned.1.call-start
  6.5 0.7 all-gather.18.cloned.1.call-update
  7.3 0.0 all-gather.8.cloned.1.call-start
  7.3 0.7 all-gather.8.cloned.1.call-update
  8.0 0.0 all-gather.10.cloned.1.call-start
  8.1 0.7 all-gather.10.cloned.1.call-update
  8.7 0.0 all-reduce.4.cloned.1.call-start
  8.8 0.0 copy-done.2
  8.8 0.0 copy-done
  8.8 0.3 fusion.10
  9.1 109.2 %all-gather.18.cloned.1.call-done = bf16[5632,512]{1,0:T(8,128)(2,1)} async-done(((bf16[1408,512]{1,0:T(8,128)(2,1)}), bf16[5632,512]{1,0:T(8,128)(2,1)}) %all-gather.18.cloned.1.call-update) | async-done | bytes 5767184 | tf_op jit(solution)/shard_map/all_gather | solution.py:72
  118.3 8.4 %copy.34 = bf16[1408,4,512]{0,2,1:T(8,128)(2,1)} copy(bf16[1408,4,512]{2,0,1:T(8,128)(2,1)} %bitcast.39) | data formatting | bytes 11534336 | tf_op jit(solution)/shard_map/reshape | solution.py:72
  126.8 98.1 %all-gather.8.cloned.1.call-done = bf16[2048,1408]{1,0:T(8,128)(2,1)} async-done(((bf16[512,1408]{1,0:T(8,128)(2,1)}), bf16[2048,1408]{1,0:T(8,128)(2,1)}) %all-gather.8.cloned.1.call-update) | async-done | bytes 5767184 | tf_op jit(solution)/shard_map/all_gather | solution.py:69
  224.9 4.5 fusion.59
  229.4 102.1 %all-gather.10.cloned.1.call-done = bf16[2048,1408]{1,0:T(8,128)(2,1)} async-done(((bf16[512,1408]{1,0:T(8,128)(2,1)}), bf16[2048,1408]{1,0:T(8,128)(2,1)}) %all-gather.10.cloned.1.call-update) | async-done | bytes 5767184 | tf_op jit(solution)/shard_map/all_gather | solution.py:70
  331.4 8.9 %convolution_convert_fusion.2 = bf16[256,2048]{1,0:T(8,128)(2,1)} fusion(bf16[1408,2048]{0,1:T(8,128)(2,1)} %bitcast.37, bf16[2048,1408]{1,0:T(8,128)(2,1)} %all-gather.10.cloned.1.call-done, f32[256,1408]{1,0:T(8,128)S(1)} %fusion.59, bf16[256,2048]{1,0:T(8,128)(2,1)S(1)} %copy-done, f32[2048]{0:T(1024)S(1)} %convert_element_type.82, ...), kind=kOutput, calls=%fused_computation.21 | convolution fusion | flops 2957574144 | bytes 15082496 | tf_op jit(solution)/shard_map/dot_general | solution.py:74
  340.3 0.0 all-reduce.4.cloned.1.call-update
  340.4 0.0 all-gather.14.cloned.1.call-start
  340.4 0.5 all-gather.14.cloned.1.call-update
  340.9 0.0 all-gather.12.cloned.1.call-start
  341.0 0.5 all-gather.12.cloned.1.call-update
  341.5 0.0 all-gather.16.cloned.1.call-start
  341.6 0.7 all-gather.16.cloned.1.call-update
  342.3 0.2 all-reduce.6.cloned.1.call-start
  342.5 0.0 copy-done.3
  342.5 0.0 copy-done.4
  342.6 0.0 copy-done.8
  342.6 0.0 copy-done.9
  342.6 32.5 %all-reduce.4.cloned.1.call-done = bf16[256,2048]{1,0:T(8,128)(2,1)} async-done(((bf16[256,2048]{1,0:T(8,128)(2,1)}), bf16[256,2048]{1,0:T(8,128)(2,1)}) %all-reduce.4.cloned.1.call-update) | async-done | bytes 1048592 | tf_op jit(solution)/shard_map/psum | solution.py:16
  375.1 1.5 fusion.2
  376.6 2.0 fusion.14
  378.5 44.1 %all-gather.14.cloned.1.call-done = bf16[2048,512]{1,0:T(8,128)(2,1)} async-done(((bf16[512,512]{1,0:T(8,128)(2,1)}), bf16[2048,512]{1,0:T(8,128)(2,1)}) %all-gather.14.cloned.1.call-update) | async-done | bytes 2097168 | tf_op jit(solution)/shard_map/all_gather | solution.py:79
  422.6 3.4 fusion.28
  426.0 0.2 reshape.107
  426.2 0.0 copy-start.1
  426.2 0.2 reshape.106
  426.4 0.3 reduce_sum.75
  426.8 0.6 multiply_reduce_fusion
  427.5 0.1 copy.47
  427.6 0.1 copy.48
  427.6 0.2 copy.36
  427.9 0.0 copy-done.1
  427.9 0.3 fusion.22
  428.2 0.2 copy.39
  428.4 40.2 %all-gather.12.cloned.1.call-done = bf16[2048,512]{1,0:T(8,128)(2,1)} async-done(((bf16[512,512]{1,0:T(8,128)(2,1)}), bf16[2048,512]{1,0:T(8,128)(2,1)}) %all-gather.12.cloned.1.call-update) | async-done | bytes 2097168 | tf_op jit(solution)/shard_map/all_gather | solution.py:78
  468.6 46.1 %all-gather.16.cloned.1.call-done = bf16[512,2048]{1,0:T(8,128)(2,1)} async-done(((bf16[512,512]{1,0:T(8,128)(2,1)}), bf16[512,2048]{1,0:T(8,128)(2,1)}) %all-gather.16.cloned.1.call-update) | async-done | bytes 2097168 | tf_op jit(solution)/shard_map/all_gather | solution.py:84
  514.6 5.7 convolution_convert_fusion
  520.3 0.0 all-reduce.6.cloned.1.call-update
  520.4 0.3 all-reduce.8.cloned.1.call-start
  520.6 0.0 copy-done.5
  520.6 0.0 copy-done.6
  520.7 34.9 %all-reduce.6.cloned.1.call-done = bf16[256,2048]{1,0:T(8,128)(2,1)} async-done(((bf16[256,2048]{1,0:T(8,128)(2,1)}), bf16[256,2048]{1,0:T(8,128)(2,1)}) %all-reduce.6.cloned.1.call-update) | async-done | bytes 1048592 | tf_op jit(solution)/shard_map/psum | solution.py:16
  555.6 1.5 fusion.5
  557.1 1.9 fusion.18
  559.0 4.5 fusion.45
  563.5 0.0 copy-start.7
  563.5 8.8 %convolution_convert_fusion.1 = bf16[256,2048]{1,0:T(8,128)(2,1)} fusion(bf16[1408,2048]{0,1:T(8,128)(2,1)} %bitcast.38, bf16[2048,1408]{1,0:T(8,128)(2,1)} %all-gather.10.cloned.1.call-done, f32[256,1408]{1,0:T(8,128)S(1)} %fusion.45, bf16[256,2048]{1,0:T(8,128)(2,1)S(1)} %get-tuple-element.6, f32[2048]{0:T(1024)S(1)} %convert_element_type.99, ...), kind=kOutput, calls=%fused_computation.20 | convolution fusion | flops 2957574144 | bytes 15082496 | tf_op jit(solution)/shard_map/dot_general | solution.py:89
  572.3 0.0 all-reduce.8.cloned.1.call-update
  572.4 0.0 copy-done.7
  572.4 36.9 %all-reduce.8.cloned.1.call-done = bf16[256,2048]{1,0:T(8,128)(2,1)} async-done(((bf16[256,2048]{1,0:T(8,128)(2,1)}), bf16[256,2048]{1,0:T(8,128)(2,1)}) %all-reduce.8.cloned.1.call-update) | async-done | bytes 1048592 | tf_op jit(solution)/shard_map/psum | solution.py:16
  609.3 1.5 fusion.7
  610.8 2.8 fusion.21
  (23 shorter events, 0.1 us)
Async XLA Ops:
  6.5 2.3 copy-start.2
  6.5 2.3 copy-start
  6.5 111.8 %all-gather.18.cloned.1.call-start = ((), (), s32[]{:S(2)}) async-start(), calls=%async_computation.8 | async-start | bytes 7208960 | tf_op jit(solution)/shard_map/all_gather | solution.py:72
  7.3 217.6 %all-gather.8.cloned.1.call-start = ((), (), s32[]{:S(2)}) async-start(), calls=%async_computation | async-start | bytes 7208960 | tf_op jit(solution)/shard_map/all_gather | solution.py:69
  8.0 323.4 %all-gather.10.cloned.1.call-start = ((), (), s32[]{:S(2)}) async-start(), calls=%async_computation.1 | async-start | bytes 7208960 | tf_op jit(solution)/shard_map/all_gather | solution.py:70
  8.7 366.3 %all-reduce.4.cloned.1.call-start = ((), (), s32[]{:S(2)}) async-start(), calls=%async_computation.2 | async-start | bytes 2097152 | tf_op jit(solution)/shard_map/psum | solution.py:16
  340.3 2.2 copy-start.3
  340.3 2.2 copy-start.4
  340.3 2.2 copy-start.8
  340.3 2.3 copy-start.9
  340.4 82.3 %all-gather.14.cloned.1.call-start = ((), (), s32[]{:S(2)}) async-start(), calls=%async_computation.4 | async-start | bytes 2621440 | tf_op jit(solution)/shard_map/all_gather | solution.py:79
  340.9 127.6 %all-gather.12.cloned.1.call-start = ((), (), s32[]{:S(2)}) async-start(), calls=%async_computation.3 | async-start | bytes 2621440 | tf_op jit(solution)/shard_map/all_gather | solution.py:78
  341.5 173.1 %all-gather.16.cloned.1.call-start = ((), (), s32[]{:S(2)}) async-start(), calls=%async_computation.5 | async-start | bytes 2621440 | tf_op jit(solution)/shard_map/all_gather | solution.py:84
  342.3 213.3 %all-reduce.6.cloned.1.call-start = ((), (), s32[]{:S(2)}) async-start(), calls=%async_computation.6 | async-start | bytes 2097152 | tf_op jit(solution)/shard_map/psum | solution.py:16
  426.2 1.6 copy-start.1
  514.6 6.0 copy-start.5
  514.6 6.0 copy-start.6
  520.4 88.9 %all-reduce.8.cloned.1.call-start = ((), (), s32[]{:S(2)}) async-start(), calls=%async_computation.7 | async-start | bytes 2097152 | tf_op jit(solution)/shard_map/psum | solution.py:16
  563.5 8.8 %copy-start.7 = (bf16[2048]{0:T(1024)(128)(2,1)S(1)}, bf16[2048]{0:T(1024)(128)(2,1)}, u32[]{:S(2)}) copy-start(bf16[2048]{0:T(1024)(128)(2,1)} %param.31) | copy-start | bytes 12292
Sparse Core Ops, SparseCore 0:
  8.9 109.3 all-gather.17
  119.9 104.9 all-gather.7
  226.5 104.9 all-gather.9
  340.5 34.5 all-reduce.3
  376.5 46.1 all-gather.13
  424.1 44.4 all-gather.11
  470.1 44.4 all-gather.15
  520.5 35.0 all-reduce.5
  572.5 36.7 all-reduce.7
